TPU v7x, 32 devices: a whole 2x2x4 slice. The times are simulated.
32 devices in a mesh: rep: 4 (over z), fs: 4 (over y, x), tp: 2 (over core).
Axes of the slice: x: 2, y: 2, z: 4, core: 2. Of those that a mesh axis runs over, the one named last changes fastest.
Arguments:
- hidden_pre: bfloat16 [8192, 4096], P(('rep', 'fs'), 'tp'), may hold values from -6 to 6
- out_grad: bfloat16 [8192, 2048], P(('rep', 'fs')), may hold values from -8 to 8
- down_weight: bfloat16 [2048, 4096], P('fs', 'tp'), may hold values from -0.09375 to 0.09375
Outputs:
- hidden_grad: bfloat16 [8192, 4096], P(('rep', 'fs'), 'tp')
- weight_grad: float32 [2048, 4096], P('fs', 'tp')
All inputs are finite; a program needn't handle non-finite values.
Results may differ from a plain program's by a relative error of at most 0.0049.
Values may be sent and summed in bfloat16 or wider, within the bound.
A program may use at most 64 MiB of HBM per device.

v0:
```python
import math
import jax
import jax.numpy as jnp
from jax import lax
from jax.sharding import PartitionSpec as P


def body(hidden_pre, out_grad, down_weight):
    rows = hidden_pre.shape[0]
    ff_local = hidden_pre.shape[1]
    back = jnp.dot(
        out_grad,
        lax.all_gather(down_weight, "fs", axis=0, tiled=True),
        preferred_element_type=jnp.float32,
    )
    positive = jnp.maximum(hidden_pre.astype(jnp.float32), 0.0)
    hidden_grad = (2.0 * positive * back).astype(jnp.bfloat16)
    act = (positive * positive).astype(jnp.bfloat16)
    partial_value = lax.dot_general(
        out_grad, act, (((0,), (0,)), ((), ())), preferred_element_type=jnp.float32
    )
    partial_value = partial_value.astype(jnp.bfloat16)
    received = lax.all_to_all(partial_value, "fs", split_axis=0, concat_axis=0, tiled=True)
    groups = lax.axis_size("fs")
    local_sum = jnp.sum(
        received.reshape(groups, received.shape[0] // groups, ff_local), axis=0, dtype=jnp.float32
    )
    total = lax.psum(local_sum, "rep")
    tokens_all = rows * lax.axis_size("rep") * groups
    weight_grad = total * (1.0 / math.sqrt(tokens_all))
    return (hidden_grad, weight_grad)


def solution(mesh):
    placed = (P(("rep", "fs"), "tp"), P(("rep", "fs"), None), P("fs", "tp"))
    return jax.shard_map(
        body,
        mesh=mesh,
        in_specs=placed,
        out_specs=(P(("rep", "fs"), "tp"), P("fs", "tp")),
        check_vma=False,
    )
```

profile of v0, /device:TPU:0, one launch (start us, length us, event | category | flops | bytes accessed | tf_op | source)
XLA Modules:
  0.0 297.2 jit_solution(1170586137731124309)
XLA Ops:
  8.0 0.0 copy-start
  8.0 0.0 all-reduce.2.cloned.1.call-start
  8.1 1.5 copy-done
  9.6 8.3 %convolution_convert_fusion = bf16[2048,2048]{0,1:T(8,128)(2,1)} fusion(bf16[512,2048]{1,0:T(8,128)(2,1)S(1)} %copy-done, bf16[512,2048]{1,0:T(8,128)(2,1)} %param.3), kind=kOutput, calls=%fused_computation.1 | convolution fusion | flops 4303355904 | bytes 12582912 | tf_op jit(solution)/shard_map/dot_general | solution.py:19
  17.9 98.5 %all_to_all.9 = bf16[4,512,2048]{2,1,0:T(8,128)(2,1)S(1)} all-to-all(bf16[4,512,2048]{2,1,0:T(8,128)(2,1)} %bitcast.6), channel_id=1, replica_groups=mesh['rep'=4,'fs'=4,'tp'=2] {'fs'}, dimensions={0} | all-to-all | bytes 16777216 | tf_op jit(solution)/shard_map/all_to_all | solution.py:23
  116.4 3.9 %convert_reduce_fusion = f32[512,2048]{1,0:T(8,128)} fusion(bf16[4,512,2048]{2,1,0:T(8,128)(2,1)S(1)} %all_to_all.9), kind=kLoop, calls=%fused_computation | loop fusion | flops 7340032 | bytes 12582912 | tf_op jit(solution)/shard_map/reduce_sum | solution.py:25
  120.3 0.0 all-reduce.2.cloned.1.call-update
  120.3 0.0 all-gather.2.cloned.1.call-start
  120.4 0.5 all-gather.2.cloned.1.call-update
  120.9 154.4 %all-reduce.2.cloned.1.call-done = f32[512,2048]{1,0:T(8,128)} async-done(((f32[512,2048]{1,0:T(8,128)}), f32[512,2048]{1,0:T(8,128)}) %all-reduce.2.cloned.1.call-update) | async-done | bytes 4194320 | tf_op jit(solution)/shard_map/psum | solution.py:28
  275.4 5.0 %broadcast_multiply_fusion = f32[512,2048]{1,0:T(8,128)} fusion(f32[512,2048]{1,0:T(8,128)} %all-reduce.2.cloned.1.call-done), kind=kLoop, calls=%fused_computation.5 | loop fusion | flops 1048576 | bytes 8388608 | tf_op jit(solution)/shard_map/mul | solution.py:30
  280.3 0.0 all-gather.2.cloned.1.call-done
  280.3 9.5 %multiply_convert_fusion.1 = bf16[512,2048]{1,0:T(8,128)(2,1)} fusion(bf16[512,2048]{1,0:T(8,128)(2,1)} %param.3, bf16[512,2048]{1,0:T(8,128)(2,1)S(1)} %copy-done, bf16[2048,2048]{1,0:T(8,128)(2,1)} %all-gather.2.cloned.1.call-done), kind=kOutput, calls=%fused_computation.3 | convolution fusion | flops 4300210176 | bytes 14680064 | tf_op jit(solution)/shard_map/dot_general | solution.py:11
Async XLA Ops:
  8.0 1.6 copy-start
  8.0 267.3 %all-reduce.2.cloned.1.call-start = ((), (), s32[]{:S(2)}) async-start(), calls=%async_computation.2 | async-start | bytes 8388608 | tf_op jit(solution)/shard_map/psum | solution.py:28
  120.3 160.0 %all-gather.2.cloned.1.call-start = ((), (), s32[]{:S(2)}) async-start(), calls=%async_computation.1 | async-start | bytes 10485760 | tf_op jit(solution)/shard_map/all_gather | solution.py:13
Sparse Core Ops, SparseCore 0:
  120.4 154.8 all-reduce.1
Sparse Core Ops, SparseCore 1:
  122.7 87.2 all-gather.1
where the time goes:
time: 297 us
  waiting for transfers between devices  155 us (52%)
  blocking collectives  98.5 us (33%)
  matrix products  17.8 us (6%)
  between operations  15.5 us (5%)
  other arithmetic  8.83 us (3%)
    psum x1, waiting for transfers between devices, body(): total = lax.psum(local_sum, 'rep')  154 us
    all_to_all x1, blocking collectives, body(): lax.all_to_all(partial_value, 'fs', split_axis=0, concat_axis=0, tiled=True)  98.5 us
    dot_general x1, matrix products, body(): jnp.dot(out_grad, lax.all_gather(down_weight, 'fs', axis=0, tiled=True),...  9.45 us
    dot_general x1, matrix products, body(): lax.dot_general(out_grad, act, (((0,), (0,)), ((), ())), preferred_elemen...  8.35 us
  transfers between devices with their start and end apart: 2, of which 1 were waited for; matrix products, arithmetic and copies ran while one was open for 2% of the time, Pallas kernels for 0%

commit v1 on v0

--- a/solution.py
+++ b/solution.py
@@ -25,7 +25,11 @@
     local_sum = jnp.sum(
         received.reshape(groups, received.shape[0] // groups, ff_local), axis=0, dtype=jnp.float32
     )
-    total = lax.psum(local_sum, "rep")
+    size = lax.axis_size("rep")
+    total, hop = (local_sum, 1)
+    while hop < size:
+        total = total + lax.ppermute(total, "rep", [(i, i ^ hop) for i in range(size)])
+        hop = 2 * hop
     tokens_all = rows * lax.axis_size("rep") * groups
     weight_grad = total * (1.0 / math.sqrt(tokens_all))
     return (hidden_grad, weight_grad)

time: 297 us -> 447 us (1.51)
  waiting for transfers between devices: 155 us -> 387 us
  blocking collectives: 98.5 us -> 0 us
  starting transfers between devices: 0.08 us -> 11 us
  other arithmetic: 8.83 us -> 15.1 us
    ppermute x0 -> x2, waiting for transfers between devices: none -> 255 us  [body(): lax.ppermute(total, 'rep', [(i, i ^ hop) for i in range(size)])]
    psum x1 -> x0, waiting for transfers between devices: 154 us -> none  [body(): total = lax.psum(local_sum, 'rep')]
    all_to_all x0 -> x1, waiting for transfers between devices: none -> 131 us  [body(): lax.all_to_all(partial_value, 'fs', split_axis=0, concat_axis=0, tiled=True)]
    all_to_all x1 -> x0, blocking collectives: 98.5 us -> none  [body(): lax.all_to_all(partial_value, 'fs', split_axis=0, concat_axis=0, tiled=True)]
    all_to_all x0 -> x1, starting transfers between devices: none -> 5.66 us  [body(): lax.all_to_all(partial_value, 'fs', split_axis=0, concat_axis=0, tiled=True)]
    ppermute x0 -> x2, starting transfers between devices: none -> 5.33 us  [body(): lax.ppermute(total, 'rep', [(i, i ^ hop) for i in range(size)])]
  transfers between devices with their start and end apart: 2 -> 4, of which waited for: 1 -> 3; matrix products, arithmetic and copies ran while one was open for 2% -> 4% of each run, Pallas kernels for 0% -> 0%
where the time goes in v1:
time: 447 us; the launch traced here: 446 us
  waiting for transfers between devices  387 us (87%)
  matrix products  17.8 us (4%)
  other arithmetic  15.1 us (3%)
  between operations  14.1 us (3%)
  starting transfers between devices  11 us (2%)
    ppermute x2, waiting for transfers between devices, body(): lax.ppermute(total, 'rep', [(i, i ^ hop) for i in range(size)])  255 us
    all_to_all x1, waiting for transfers between devices, body(): lax.all_to_all(partial_value, 'fs', split_axis=0, concat_axis=0, tiled=True)  131 us
    dot_general x1, matrix products, body(): jnp.dot(out_grad, lax.all_gather(down_weight, 'fs', axis=0, tiled=True),...  9.45 us
  transfers between devices with their start and end apart: 4, of which 3 were waited for; matrix products, arithmetic and copies ran while one was open for 4% of the time, Pallas kernels for 0%

profile of v1, /device:TPU:0, one launch (start us, length us, event | category | flops | bytes accessed | tf_op | source)
XLA Modules:
  0.0 446.3 jit_solution(14446443577105886237)
XLA Ops:
  7.2 0.0 copy-start
  7.2 1.6 copy-done
  8.8 8.4 %convolution_convert_fusion = bf16[2048,2048]{0,1:T(8,128)(2,1)} fusion(bf16[512,2048]{1,0:T(8,128)(2,1)S(1)} %copy-done, bf16[512,2048]{1,0:T(8,128)(2,1)} %param.3), kind=kOutput, calls=%fused_computation.1 | convolution fusion | flops 4303355904 | bytes 12582912 | tf_op jit(solution)/shard_map/dot_general | solution.py:19
  17.1 5.7 %all-to-all-start = ((bf16[4,512,2048]{2,1,0:T(8,128)(2,1)}), bf16[4,512,2048]{2,1,0:T(8,128)(2,1)}, u32[]{:S(2)}, u32[]{:S(2)}) async-start(bf16[4,512,2048]{2,1,0:T(8,128)(2,1)} %bitcast.6), calls=%async_computation | async-start | bytes 16777216 | tf_op jit(solution)/shard_map/all_to_all | solution.py:23
  22.8 0.0 all-gather.2.cloned.1.call-start
  22.8 0.7 all-gather.2.cloned.1.call-update
  23.5 130.7 %all-to-all-done = bf16[4,512,2048]{2,1,0:T(8,128)(2,1)} async-done(((bf16[4,512,2048]{2,1,0:T(8,128)(2,1)}), bf16[4,512,2048]{2,1,0:T(8,128)(2,1)}, u32[]{:S(2)}, u32[]{:S(2)}) %all-to-all-start) | async-done | bytes 8388640 | tf_op jit(solution)/shard_map/all_to_all | solution.py:23
  154.2 5.7 %convert_reduce_fusion = f32[512,2048]{1,0:T(8,128)S(1)} fusion(bf16[4,512,2048]{2,1,0:T(8,128)(2,1)} %all-to-all-done), kind=kLoop, calls=%fused_computation | loop fusion | flops 7340032 | bytes 12582912 | tf_op jit(solution)/shard_map/reduce_sum | solution.py:25
  159.9 2.5 collective-permute-start
  162.4 87.7 %collective-permute-done = f32[512,2048]{1,0:T(8,128)S(1)} collective-permute-done((f32[512,2048]{1,0:T(8,128)S(1)}, f32[512,2048]{1,0:T(8,128)S(1)}, u32[]{:S(2)}, u32[]{:S(2)}) %collective-permute-start) | collective-permute-done | bytes 4194336 | tf_op jit(solution)/shard_map/ppermute | solution.py:31
  250.1 2.8 add.6
  252.8 2.8 collective-permute-start.1
  255.7 0.0 all-gather.2.cloned.1.call-done
  255.7 9.5 %multiply_convert_fusion.1 = bf16[512,2048]{1,0:T(8,128)(2,1)} fusion(bf16[512,2048]{1,0:T(8,128)(2,1)} %param.3, bf16[512,2048]{1,0:T(8,128)(2,1)S(1)} %copy-done, bf16[2048,2048]{1,0:T(8,128)(2,1)} %all-gather.2.cloned.1.call-done), kind=kOutput, calls=%fused_computation.4 | convolution fusion | flops 4300210176 | bytes 14680064 | tf_op jit(solution)/shard_map/dot_general | solution.py:11
  265.1 167.6 %collective-permute-done.1 = f32[512,2048]{1,0:T(8,128)} collective-permute-done((f32[512,2048]{1,0:T(8,128)}, f32[512,2048]{1,0:T(8,128)}, u32[]{:S(2)}, u32[]{:S(2)}) %collective-permute-start.1) | collective-permute-done | bytes 4194336 | tf_op jit(solution)/shard_map/ppermute | solution.py:31
  432.8 6.7 %add_multiply_fusion = f32[512,2048]{1,0:T(8,128)} fusion(f32[512,2048]{1,0:T(8,128)} %add.6, f32[512,2048]{1,0:T(8,128)} %collective-permute-done.1), kind=kLoop, calls=%fused_computation.2 | loop fusion | flops 2097152 | bytes 12582912 | tf_op jit(solution)/shard_map/mul | solution.py:34
Async XLA Ops:
  7.2 1.6 copy-start
  17.1 137.1 %all-to-all-start = ((bf16[4,512,2048]{2,1,0:T(8,128)(2,1)}), bf16[4,512,2048]{2,1,0:T(8,128)(2,1)}, u32[]{:S(2)}, u32[]{:S(2)}) async-start(bf16[4,512,2048]{2,1,0:T(8,128)(2,1)} %bitcast.6), calls=%async_computation | async-start | bytes 16777216 | tf_op jit(solution)/shard_map/all_to_all | solution.py:23
  22.8 232.9 %all-gather.2.cloned.1.call-start = ((), (), s32[]{:S(2)}) async-start(), calls=%async_computation.1 | async-start | bytes 10485760 | tf_op jit(solution)/shard_map/all_gather | solution.py:13
  159.9 90.2 %collective-permute-start = (f32[512,2048]{1,0:T(8,128)S(1)}, f32[512,2048]{1,0:T(8,128)S(1)}, u32[]{:S(2)}, u32[]{:S(2)}) collective-permute-start(f32[512,2048]{1,0:T(8,128)S(1)} %convert_reduce_fusion), channel_id=1, source_target_pairs={{0,8},{8,0},{16,24},{24,16},{1,9},{9,1},{17,25},{25,17},{2,10},{10... | collective-permute-start | bytes 12582920 | tf_op jit(solution)/shard_map/ppermute | solution.py:31
  252.8 179.9 %collective-permute-start.1 = (f32[512,2048]{1,0:T(8,128)}, f32[512,2048]{1,0:T(8,128)}, u32[]{:S(2)}, u32[]{:S(2)}) collective-permute-start(f32[512,2048]{1,0:T(8,128)} %add.6), channel_id=1, source_target_pairs={{0,16},{8,24},{16,0},{24,8},{1,17},{9,25},{17,1},{25,9},{2,18},{10... | collective-permute-start | bytes 12582920 | tf_op jit(solution)/shard_map/ppermute | solution.py:31
Sparse Core Ops, SparseCore 0:
  25.5 158.7 all-gather.1
